TPU v7x, 512 devices: a whole 4x8x8 slice. The times are simulated.
512 devices in a mesh: rep: 2 (over z_hi), fs: 32 (over z_lo, y), tp: 8 (over x, core).
Axes of the slice: x: 4, y: 8, z: 8 (z_hi: 2, z_lo: 4; z = z_hi * 4 + z_lo), core: 2. Of those that a mesh axis runs over, the one named last changes fastest.
Arguments:
- tokens: bfloat16 [20480, 2048], P(('rep', 'fs')), may hold values from -6 to 6
- gate_weight: float32 [2048, 5120], P('fs', 'tp'), may hold values from -0.125 to 0.125
- up_weight: float32 [2048, 5120], P('fs', 'tp'), may hold values from -0.125 to 0.125
- down_weight: float32 [2048, 5120], P('fs', 'tp'), may hold values from -0.078125 to 0.078125
- value_weight: float32 [2048, 2048], P('fs', 'tp'), may hold values from -0.125 to 0.125
- glu_weight: float32 [2048, 2048], P('fs', 'tp'), may hold values from -0.125 to 0.125
- out_weight: float32 [2048, 2048], P('fs', 'tp'), may hold values from -0.125 to 0.125
- gate_scale: float32 [5120], P('tp'), may hold values from 0.1 to 1.9
- up_scale: float32 [5120], P('tp'), may hold values from 0.5 to 2
- down_scale: float32 [2048], P('fs'), may hold values from 1 to 4
- value_scale: float32 [2048], P('tp'), may hold values from 0.2 to 3.4
- glu_scale: float32 [2048], P('tp'), may hold values from 0.1 to 1.9
- out_scale: float32 [2048], P('fs'), may hold values from 1 to 4
- conv_kernel: float32 [31, 2048], P(None, 'tp'), may hold values from -1 to 1
- norm_gain: float32 [2048], P('tp'), may hold values from 0.1 to 1.9
- first_gain: float32 [2048], replicated, may hold values from 0.1 to 1.9
- conv_gain: float32 [2048], replicated, may hold values from 0.1 to 1.9
- second_gain: float32 [2048], replicated, may hold values from 0.1 to 1.9
Outputs:
- result: bfloat16 [20480, 2048], P(('rep', 'fs'))
All inputs are finite; a program needn't handle non-finite values.
Results may differ from a plain program's by a relative error of at most 0.02.
Values may be sent and summed in bfloat16 or wider, within the bound.
No kernel may reach another device: no remote copies, remote signals or barrier semaphores. Data moves between devices by JAX's collectives and lax.ppermute only.
A program may use at most 64 MiB of HBM per device.

v0:
```python
import jax
import jax.numpy as jnp
from jax import lax
from jax.sharding import PartitionSpec as P

D = 2048
EPSILON = 1e-06


def split_up(shard, dim, size):
    before, after = (shard.shape[:dim], shard.shape[dim + 1 :])
    return jnp.moveaxis(shard.reshape(*before, size, -1, *after), dim, 0)


def sum_at_owner(shard, axis, dim):
    size = lax.axis_size(axis)
    parts = lax.all_to_all(split_up(shard, dim, size), axis, 0, 0, tiled=True)
    return jnp.sum(parts.astype(jnp.float32), axis=0)


def side_by_side(arrays, axis, dim, along):
    widths = [a.shape[along] for a in arrays]
    both = jnp.concatenate(arrays, axis=along)
    out = lax.all_gather(both, axis, axis=dim, tiled=True)
    return tuple(jnp.split(out, [sum(widths[:k]) for k in range(1, len(widths))], axis=along))


def rows_first(arrays, axis, dims):
    turned = [jnp.moveaxis(a, dim, 0) for a, dim in zip(arrays, dims)]
    both = jnp.concatenate([t.reshape(len(t), -1) for t in turned], axis=1)
    out, at, outs = (lax.all_gather(both, axis, axis=0, tiled=True), 0, [])
    for t, dim in zip(turned, dims):
        slab = out[:, at : at + t[0].size].reshape(-1, *t.shape[1:])
        outs.append(jnp.moveaxis(slab, 0, dim))
        at += t[0].size
    return tuple(outs)


def in_order(parts, dim):
    shape = list(parts.shape[1:])
    shape[dim] *= parts.shape[0]
    return jnp.moveaxis(parts, 0, dim).reshape(shape)


def copy_for_each(shard, axis):
    size = lax.axis_size(axis)
    return lax.all_to_all(
        jnp.broadcast_to(shard[None], (size, *shard.shape)), axis, 0, 0, tiled=True
    )


def collect(shard, axis, dim):
    return in_order(copy_for_each(shard, axis), dim)


def over_copies(shard, axis):
    return copy_for_each(shard, axis).sum(axis=0)


def in_one(arrays, axis):
    ravelled, at, outs = (jnp.concatenate([a.reshape(-1) for a in arrays]), 0, [])
    running = over_copies(ravelled, axis)
    for a in arrays:
        outs.append(running[at : at + a.size].reshape(a.shape))
        at += a.size
    return tuple(outs)


def rms_rows(rows, gains):
    values = rows.astype(jnp.float32)
    scaled = values * lax.rsqrt(jnp.mean(values * values, axis=-1, keepdims=True) + EPSILON)
    return (scaled * gains).astype(jnp.bfloat16)


def gated_hidden(normed, gate_full, up_full, gate_scale, up_scale):
    gate_part = jnp.dot(normed, gate_full, preferred_element_type=jnp.float32) * gate_scale
    upward = jnp.dot(normed, up_full, preferred_element_type=jnp.float32) * up_scale
    return (jax.nn.silu(gate_part) * upward).astype(jnp.bfloat16)


def causal_depthwise(inputs, kernel):
    taps = kernel.shape[0]
    length = inputs.shape[0]
    padded = jnp.concatenate(
        [jnp.zeros((taps - 1, inputs.shape[1]), jnp.float32), inputs.astype(jnp.float32)], axis=0
    )
    total = jnp.zeros((length, inputs.shape[1]), jnp.float32)
    for offset in range(taps):
        total = total + kernel[offset] * padded[offset : offset + length]
    return total


def branch_sum(active, weight_rows):
    return sum_at_owner(
        lax.dot_general(
            active, weight_rows, (((1,), (1,)), ((), ())), preferred_element_type=jnp.float32
        ).astype(jnp.bfloat16),
        "tp",
        0,
    )


def local(
    tokens,
    gate_weight,
    up_weight,
    down_weight,
    value_weight,
    glu_weight,
    out_weight,
    gate_scale,
    up_scale,
    down_scale,
    value_scale,
    glu_scale,
    out_scale,
    conv_kernel,
    norm_gain,
    first_gain,
    conv_gain,
    second_gain,
):
    gate_cast = gate_weight.astype(jnp.bfloat16)
    up_cast = up_weight.astype(jnp.bfloat16)
    down_cast = down_weight.astype(jnp.bfloat16)
    value_cast = value_weight.astype(jnp.bfloat16)
    glu_cast = glu_weight.astype(jnp.bfloat16)
    out_cast = out_weight.astype(jnp.bfloat16)
    gate_full, up_full, down_full, value_full, glu_full, out_full = side_by_side(
        (gate_cast, up_cast, down_cast, value_cast, glu_cast, out_cast), "fs", 0, 1
    )
    down_rows, out_rows = rows_first((down_scale, out_scale), "fs", (0, 0))
    members = lax.axis_size("tp")
    own_rows = tokens.shape[0] // members
    first_row = lax.axis_index("tp") * own_rows
    hidden = gated_hidden(rms_rows(tokens, first_gain), gate_full, up_full, gate_scale, up_scale)
    own_tokens = lax.dynamic_slice_in_dim(tokens, first_row, own_rows, 0)
    after_first = (
        own_tokens.astype(jnp.float32) + 0.5 * down_rows * branch_sum(hidden, down_full)
    ).astype(jnp.bfloat16)
    rows = collect(rms_rows(after_first, conv_gain), "tp", 0)
    value_part = jnp.dot(rows, value_full, preferred_element_type=jnp.float32) * value_scale
    gate_part = jnp.dot(rows, glu_full, preferred_element_type=jnp.float32) * glu_scale
    glu_in = (value_part * jax.nn.sigmoid(gate_part)).astype(jnp.bfloat16)
    mixed = causal_depthwise(glu_in, conv_kernel)
    row_sums, row_squares = in_one((jnp.sum(mixed, axis=1), jnp.sum(mixed * mixed, axis=1)), "tp")
    mean_rows = (row_sums / D)[:, None]
    square_rows = (row_squares / D)[:, None]
    normalized = (
        (mixed - mean_rows) * lax.rsqrt(square_rows - mean_rows * mean_rows + EPSILON) * norm_gain
    )
    active = jax.nn.silu(normalized).astype(jnp.bfloat16)
    after_conv = (after_first.astype(jnp.float32) + out_rows * branch_sum(active, out_full)).astype(
        jnp.bfloat16
    )
    hidden = gated_hidden(
        collect(rms_rows(after_conv, second_gain), "tp", 0),
        gate_full,
        up_full,
        gate_scale,
        up_scale,
    )
    after_second = (
        after_conv.astype(jnp.float32) + 0.5 * down_rows * branch_sum(hidden, down_full)
    ).astype(jnp.bfloat16)
    return collect(after_second, "tp", 0)


def solution(mesh):
    placed = (
        P(("rep", "fs"), None),
        P("fs", "tp"),
        P("fs", "tp"),
        P("fs", "tp"),
        P("fs", "tp"),
        P("fs", "tp"),
        P("fs", "tp"),
        P("tp"),
        P("tp"),
        P("fs"),
        P("tp"),
        P("tp"),
        P("fs"),
        P(None, "tp"),
        P("tp"),
        P(),
        P(),
        P(),
    )
    return jax.shard_map(
        local, mesh=mesh, in_specs=placed, out_specs=P(("rep", "fs"), None), check_vma=False
    )
```

profile of v0, /device:TPU:1, one launch (start us, length us, event | category | flops | bytes accessed | tf_op | source)
XLA Modules:
  0.0 425.5 jit_solution(13172832336793089133)
XLA Ops:
  6.5 0.0 copy-start
  6.5 0.0 copy-start.7
  6.5 0.0 copy-start.8
  6.5 0.0 all-gather.3.cloned.1.call-start
  6.5 1.0 convert_dynamic-update-slice_fusion.2
  7.6 0.9 convert_dynamic-update-slice_fusion.1
  8.5 0.9 convert_dynamic-update-slice_fusion
  9.4 0.8 convert_dynamic-update-slice_fusion.5
  10.3 0.8 convert_dynamic-update-slice_fusion.4
  11.1 0.8 convert_dynamic-update-slice_fusion.3
  12.0 0.0 copy-start.1
  12.0 0.7 copy-done.1
  12.7 0.0 all-gather.3.cloned.1.call-update
  12.7 1.7 fusion
  14.4 0.0 copy-start.9
  14.4 158.1 %all-gather.3.cloned.1.call-done = bf16[2048,2688]{1,0:T(8,128)(2,1)} async-done(((bf16[64,2688]{1,0:T(8,128)(2,1)}), bf16[2048,2688]{1,0:T(8,128)(2,1)}) %all-gather.3.cloned.1.call-update) | async-done | bytes 11010064 | tf_op jit(solution)/shard_map/all_gather | solution.py:24
  172.5 0.0 copy-done
  172.5 0.0 copy-done.7
  172.5 0.0 copy-done.8
  172.5 3.0 fusion.13
  175.5 0.0 copy-done.9
  175.5 6.3 %convolution_convert_fusion.2 = bf16[320,2048]{1,0:T(8,128)(2,1)} fusion(bf16[2048,2688]{1,0:T(8,128)(2,1)} %all-gather.3.cloned.1.call-done, f32[320,640]{1,0:T(8,128)S(1)} %fusion.13, f32[640]{0:T(1024)S(1)} %copy-done.9, bf16[320,2048]{1,0:T(8,128)(2,1)S(1)} %copy-done, f32[2048]{0:T(1024)S(1)} %copy-done.7, f32[320]{0:T(512)S(1)} %add_rsqrt_fusion.1), kind=kOutput, calls=%fused_computation.4 | convolution fusion | flops 1682432000 | bytes 8695552 | tf_op jit(solution)/shard_map/dot_general | solution.py:95
  181.8 23.9 %all-to-all-start = ((bf16[8,40,2048]{2,1,0:T(8,128)(2,1)}), bf16[8,40,2048]{2,1,0:T(8,128)(2,1)S(1)}, u32[]{:S(2)}, u32[]{:S(2)}) async-start(bf16[8,40,2048]{2,1,0:T(8,128)(2,1)} %bitcast.52), calls=%async_computation | async-start | bytes 2621440 | tf_op jit(solution)/shard_map/all_to_all | solution.py:17
  205.7 0.0 copy-done.5
  205.7 0.0 copy-done.6
  205.7 62.5 %all-gather = f32[32,64,2]{1,2,0:T(2,128)S(1)} all-gather(f32[1,64,2]{1,2,0:T(2,128)S(1)} %maximum_bitcast_fusion), channel_id=1, replica_groups=mesh['rep'=2,'fs'=32,'tp'=8] {'fs'}, dimensions={0}, use_global_device_ids=true | all-gather | bytes 16896 | tf_op jit(solution)/shard_map/all_gather | solution.py:31
  268.2 0.1 reshape.89
  268.3 0.0 all-to-all-done
  268.3 0.2 convert_reduce_fusion.2
  268.5 0.0 copy-start.2
  268.5 0.0 copy-start.10
  268.5 0.2 fusion.68
  268.7 0.0 copy-done.3
  268.7 0.1 fusion.70
  268.8 1.2 broadcast_in_dim.8
  270.0 19.0 %all-to-all-start.1 = ((bf16[8,40,2048]{2,1,0:T(8,128)(2,1)}), bf16[8,40,2048]{2,1,0:T(8,128)(2,1)S(1)}, u32[]{:S(2)}, u32[]{:S(2)}) async-start(bf16[8,40,2048]{2,1,0:T(8,128)(2,1)} %broadcast_in_dim.8), calls=%async_computation.1 | async-start | bytes 2621440 | tf_op jit(solution)/shard_map/all_to_all | solution.py:47
  289.0 0.0 copy-done.2
  289.1 17.7 %all-to-all-done.1 = bf16[8,40,2048]{2,1,0:T(8,128)(2,1)S(1)} async-done(((bf16[8,40,2048]{2,1,0:T(8,128)(2,1)}), bf16[8,40,2048]{2,1,0:T(8,128)(2,1)S(1)}, u32[]{:S(2)}, u32[]{:S(2)}) %all-to-all-start.1) | async-done | bytes 1310752 | tf_op jit(solution)/shard_map/all_to_all | solution.py:47
  306.8 0.0 copy-done.10
  306.8 1.8 fusion.40
  308.6 0.0 copy-done.11
  308.6 0.0 copy-start.12
  308.6 1.8 fusion.43
  310.4 1.3 fusion.138
  311.7 0.1 pad_maximum_fusion
  311.8 8.0 %all_to_all.36 = f32[8,1,640]{2,1,0:T(1,128)S(1)} all-to-all(f32[8,1,640]{2,1,0:T(1,128)S(1)} %broadcast_in_dim.9), channel_id=1, replica_groups=mesh['rep'=2,'fs'=32,'tp'=8] {'tp'}, dimensions={0} | all-to-all | bytes 40960 | tf_op jit(solution)/shard_map/all_to_all | solution.py:47
  319.8 0.1 slice_multiply_fusion.1
  319.9 0.0 copy-done.12
  319.9 1.8 convolution_convert_fusion.1
  321.7 0.0 copy-start.4
  321.8 20.9 %all_to_all.37 = bf16[8,40,2048]{2,1,0:T(8,128)(2,1)S(1)} all-to-all(bf16[8,40,2048]{2,1,0:T(8,128)(2,1)S(1)} %bitcast.53), channel_id=1, replica_groups=mesh['rep'=2,'fs'=32,'tp'=8] {'tp'}, dimensions={0} | all-to-all | bytes 2621440 | tf_op jit(solution)/shard_map/all_to_all | solution.py:17
  342.6 0.2 convert_reduce_fusion.1
  342.8 0.2 fusion.72
  343.0 0.0 copy-done.4
  343.0 0.1 fusion.74
  343.1 0.1 broadcast_in_dim.10
  343.3 21.2 %all_to_all.38 = bf16[8,40,2048]{2,1,0:T(8,128)(2,1)S(1)} all-to-all(bf16[8,40,2048]{2,1,0:T(8,128)(2,1)S(1)} %broadcast_in_dim.10), channel_id=1, replica_groups=mesh['rep'=2,'fs'=32,'tp'=8] {'tp'}, dimensions={0} | all-to-all | bytes 2621440 | tf_op jit(solution)/shard_map/all_to_all | solution.py:47
  364.5 2.9 fusion.16
  367.4 6.3 %convolution_convert_fusion = bf16[320,2048]{1,0:T(8,128)(2,1)} fusion(bf16[2048,2688]{1,0:T(8,128)(2,1)} %all-gather.3.cloned.1.call-done, bf16[320,2048]{1,0:T(8,128)(2,1)S(1)} %bitcast.55, f32[320,640]{1,0:T(8,128)S(1)} %fusion.16, f32[640]{0:T(1024)S(1)} %copy-done.9), kind=kOutput, calls=%fused_computation.2 | convolution fusion | flops 1679810560 | bytes 8686080 | tf_op jit(solution)/shard_map/dot_general | solution.py:95
  373.8 22.3 %all_to_all.39 = bf16[8,40,2048]{2,1,0:T(8,128)(2,1)S(1)} all-to-all(bf16[8,40,2048]{2,1,0:T(8,128)(2,1)} %bitcast.56), channel_id=1, replica_groups=mesh['rep'=2,'fs'=32,'tp'=8] {'tp'}, dimensions={0} | all-to-all | bytes 2621440 | tf_op jit(solution)/shard_map/all_to_all | solution.py:17
  396.0 0.2 convert_reduce_fusion
  396.3 0.1 broadcast_in_dim.11
  396.4 21.2 %all_to_all.40 = bf16[8,40,2048]{2,1,0:T(8,128)(2,1)S(1)} all-to-all(bf16[8,40,2048]{2,1,0:T(8,128)(2,1)S(1)} %broadcast_in_dim.11), channel_id=1, replica_groups=mesh['rep'=2,'fs'=32,'tp'=8] {'tp'}, dimensions={0} | all-to-all | bytes 2621440 | tf_op jit(solution)/shard_map/all_to_all | solution.py:47
  417.6 1.1 copy.33
  (15 shorter events, 0.2 us)
Async XLA Ops:
  6.5 166.0 %copy-start = (bf16[320,2048]{1,0:T(8,128)(2,1)S(1)}, bf16[320,2048]{1,0:T(8,128)(2,1)}, u32[]{:S(2)}) copy-start(bf16[320,2048]{1,0:T(8,128)(2,1)} %param.18) | copy-start | bytes 3932164
  6.5 166.0 %copy-start.7 = (f32[2048]{0:T(1024)S(1)}, f32[2048]{0:T(1024)}, u32[]{:S(2)}) copy-start(f32[2048]{0:T(1024)} %param.33) | copy-start | bytes 24580
  6.5 166.0 %copy-start.8 = (f32[640]{0:T(1024)S(1)}, f32[640]{0:T(1024)}, u32[]{:S(2)}) copy-start(f32[640]{0:T(1024)} %param.25) | copy-start | bytes 7684
  6.5 165.9 %all-gather.3.cloned.1.call-start = ((), (), s32[]{:S(2)}) async-start(), calls=%async_computation.7 | async-start | bytes 11354112 | tf_op jit(solution)/shard_map/all_gather | solution.py:24
  12.0 0.7 copy-start.1
  14.4 161.1 %copy-start.9 = (f32[640]{0:T(1024)S(1)}, f32[640]{0:T(1024)}, u32[]{:S(2)}) copy-start(f32[640]{0:T(1024)} %param.26) | copy-start | bytes 7684
  181.8 23.9 %copy-start.5 = (f32[64]{0:T(128)S(1)}, f32[64]{0:T(128)}, u32[]{:S(2)}) copy-start(f32[64]{0:T(128)} %param.30) | copy-start | bytes 772
  181.8 23.9 %copy-start.6 = (f32[64]{0:T(128)S(1)}, f32[64]{0:T(128)}, u32[]{:S(2)}) copy-start(f32[64]{0:T(128)} %param.27) | copy-start | bytes 772
  181.8 86.9 %copy-start.3 = (f32[2048]{0:T(1024)S(1)}, f32[2048]{0:T(1024)}, u32[]{:S(2)}) copy-start(f32[2048]{0:T(1024)} %param.34) | copy-start | bytes 24580
  181.8 86.5 %all-to-all-start = ((bf16[8,40,2048]{2,1,0:T(8,128)(2,1)}), bf16[8,40,2048]{2,1,0:T(8,128)(2,1)S(1)}, u32[]{:S(2)}, u32[]{:S(2)}) async-start(bf16[8,40,2048]{2,1,0:T(8,128)(2,1)} %bitcast.52), calls=%async_computation | async-start | bytes 2621440 | tf_op jit(solution)/shard_map/all_to_all | solution.py:17
  268.5 20.5 %copy-start.2 = (f32[31,256]{1,0:T(8,128)S(1)}, f32[31,256]{1,0:T(8,128)}, u32[]{:S(2)}) copy-start(f32[31,256]{1,0:T(8,128)} %param.31) | copy-start | bytes 95236
  268.5 38.3 %copy-start.10 = (f32[256]{0:T(256)S(1)}, f32[256]{0:T(256)}, u32[]{:S(2)}) copy-start(f32[256]{0:T(256)} %param.29) | copy-start | bytes 3076
  270.0 36.8 %all-to-all-start.1 = ((bf16[8,40,2048]{2,1,0:T(8,128)(2,1)}), bf16[8,40,2048]{2,1,0:T(8,128)(2,1)S(1)}, u32[]{:S(2)}, u32[]{:S(2)}) async-start(bf16[8,40,2048]{2,1,0:T(8,128)(2,1)} %broadcast_in_dim.8), calls=%async_computation.1 | async-start | bytes 2621440 | tf_op jit(solution)/shard_map/all_to_all | solution.py:47
  306.8 1.8 copy-start.11
  308.6 11.3 %copy-start.12 = (f32[256]{0:T(256)S(1)}, f32[256]{0:T(256)}, u32[]{:S(2)}) copy-start(f32[256]{0:T(256)} %param.32) | copy-start | bytes 3076
  321.7 21.3 %copy-start.4 = (f32[2048]{0:T(1024)S(1)}, f32[2048]{0:T(1024)}, u32[]{:S(2)}) copy-start(f32[2048]{0:T(1024)} %param.35) | copy-start | bytes 24580
Sparse Core Ops, SparseCore 0:
  12.9 159.5 all-gather.2
where the time goes:
time: 426 us
  waiting for transfers between devices  176 us (41%)
  blocking collectives  156 us (37%)
  starting transfers between devices  42.9 us (10%)
  matrix products  23.9 us (6%)
  between operations  13.6 us (3%)
  other arithmetic  9.87 us (2%)
    all_gather x1, waiting for transfers between devices, side_by_side(): out = lax.all_gather(both, axis, axis=dim, tiled=True)  158 us
    all_gather x1, blocking collectives, rows_first(): out, at, outs = (lax.all_gather(both, axis, axis=0, tiled=True), 0, [])  62.5 us
    all_to_all x3, blocking collectives, copy_for_each(): lax.all_to_all(jnp.broadcast_to(shard[None], (size, *shard.shape)), axis,...  50.4 us
    all_to_all x2, blocking collectives, sum_at_owner(): parts = lax.all_to_all(split_up(shard, dim, size), axis, 0, 0, tiled=True)  43.1 us
    all_to_all x1, starting transfers between devices, sum_at_owner(): parts = lax.all_to_all(split_up(shard, dim, size), axis, 0, 0, tiled=True)  23.9 us
    all_to_all x1, starting transfers between devices, copy_for_each(): lax.all_to_all(jnp.broadcast_to(shard[None], (size, *shard.shape)), axis,...  19 us
    all_to_all x1, waiting for transfers between devices, copy_for_each(): lax.all_to_all(jnp.broadcast_to(shard[None], (size, *shard.shape)), axis,...  17.7 us
    dot_general x3, matrix products, branch_sum(): lax.dot_general(active, weight_rows, (((1,), (1,)), ((), ())), preferred_...  14.5 us
  transfers between devices with their start and end apart: 3, of which 2 were waited for; matrix products, arithmetic and copies ran while one was open for 0% of the time, Pallas kernels for 0%

commit v1 on v0

--- a/solution.py
+++ b/solution.py
@@ -28,7 +28,13 @@
 def rows_first(arrays, axis, dims):
     turned = [jnp.moveaxis(a, dim, 0) for a, dim in zip(arrays, dims)]
     both = jnp.concatenate([t.reshape(len(t), -1) for t in turned], axis=1)
-    out, at, outs = (lax.all_gather(both, axis, axis=0, tiled=True), 0, [])
+    out, at, outs = (
+        jnp.concatenate(
+            lax.all_to_all(jnp.stack([both] * lax.axis_size(axis)), axis, 0, 0), axis=0
+        ),
+        0,
+        [],
+    )
     for t, dim in zip(turned, dims):
         slab = out[:, at : at + t[0].size].reshape(-1, *t.shape[1:])
         outs.append(jnp.moveaxis(slab, 0, dim))

time: 426 us -> 366 us (0.86)
  blocking collectives: 156 us -> 92.5 us
    all_gather x1 -> x0, blocking collectives: 62.5 us -> none  [rows_first(): out, at, outs = (lax.all_gather(both, axis, axis=0, tiled=True), 0, [])]
    all_to_all x1, waiting for transfers between devices: 0.01 us -> 16.5 us  [sum_at_owner(): parts = lax.all_to_all(split_up(shard, dim, size), axis, 0, 0, tiled=True)]
    all_gather x1, waiting for transfers between devices: 158 us -> 143 us  [side_by_side(): out = lax.all_gather(both, axis, axis=dim, tiled=True)]
    all_to_all x1, starting transfers between devices: 19 us -> 4.44 us  [copy_for_each(): lax.all_to_all(jnp.broadcast_to(shard[None], (size, *shard.shape)), axis,...]
    all_to_all x0 -> x1, starting transfers between devices: none -> 13.5 us  [rows_first(): lax.all_to_all(jnp.stack([both] * lax.axis_size(axis)), axis, 0, 0)]
  transfers between devices with their start and end apart: 3 -> 4, of which waited for: 2 -> 3; matrix products, arithmetic and copies ran while one was open for 0% -> 4% of each run, Pallas kernels for 0% -> 0%
where the time goes in v1:
time: 366 us; the launch traced here: 365 us
  waiting for transfers between devices  177 us (48%)
  blocking collectives  92.5 us (25%)
  starting transfers between devices  41.7 us (11%)
  matrix products  23.8 us (7%)
  between operations  13.6 us (4%)
  other arithmetic  11.1 us (3%)
  local copies, waits for them, and re-layouts  4.73 us (1%)
    all_gather x1, waiting for transfers between devices, side_by_side(): out = lax.all_gather(both, axis, axis=dim, tiled=True)  143 us
    all_to_all x3, blocking collectives, copy_for_each(): lax.all_to_all(jnp.broadcast_to(shard[None], (size, *shard.shape)), axis,...  50.4 us
    all_to_all x2, blocking collectives, sum_at_owner(): parts = lax.all_to_all(split_up(shard, dim, size), axis, 0, 0, tiled=True)  42.1 us
    all_to_all x1, starting transfers between devices, sum_at_owner(): parts = lax.all_to_all(split_up(shard, dim, size), axis, 0, 0, tiled=True)  23.8 us
    all_to_all x1, waiting for transfers between devices, copy_for_each(): lax.all_to_all(jnp.broadcast_to(shard[None], (size, *shard.shape)), axis,...  17.8 us
    all_to_all x1, waiting for transfers between devices, sum_at_owner(): parts = lax.all_to_all(split_up(shard, dim, size), axis, 0, 0, tiled=True)  16.5 us
    dot_general x3, matrix products, branch_sum(): lax.dot_general(active, weight_rows, (((1,), (1,)), ((), ())), preferred_...  13.5 us
    all_to_all x1, starting transfers between devices, rows_first(): lax.all_to_all(jnp.stack([both] * lax.axis_size(axis)), axis, 0, 0)  13.5 us
  transfers between devices with their start and end apart: 4, of which 3 were waited for; matrix products, arithmetic and copies ran while one was open for 4% of the time, Pallas kernels for 0%

profile of v1, /device:TPU:1, one launch (start us, length us, event | category | flops | bytes accessed | tf_op | source)
XLA Modules:
  0.0 365.0 jit_solution(1340345547208891409)
XLA Ops:
  6.5 0.0 copy-start
  6.5 0.0 all-gather.2.cloned.1.call-start
  6.5 1.0 convert_dynamic-update-slice_fusion.2
  7.6 0.9 convert_dynamic-update-slice_fusion.1
  8.5 0.9 convert_dynamic-update-slice_fusion
  9.4 0.8 convert_dynamic-update-slice_fusion.5
  10.3 0.8 convert_dynamic-update-slice_fusion.4
  11.1 0.8 convert_dynamic-update-slice_fusion.3
  12.0 0.7 copy-done.1
  12.7 0.0 all-gather.2.cloned.1.call-update
  12.7 0.7 pad_maximum_fusion.1
  13.4 0.7 reshape.94
  14.1 13.5 %all-to-all-start = ((f32[32,1,128]{2,1,0:T(1,128)}), f32[32,1,128]{2,1,0:T(1,128)S(1)}, u32[]{:S(2)}, u32[]{:S(2)}) async-start(f32[32,1,128]{2,1,0:T(1,128)} %reshape.94), calls=%async_computation | async-start | bytes 32768 | tf_op jit(solution)/shard_map/all_to_all | solution.py:33
  27.6 1.7 fusion
  29.3 143.2 %all-gather.2.cloned.1.call-done = bf16[2048,2688]{1,0:T(8,128)(2,1)} async-done(((bf16[64,2688]{1,0:T(8,128)(2,1)}), bf16[2048,2688]{1,0:T(8,128)(2,1)}) %all-gather.2.cloned.1.call-update) | async-done | bytes 11010064 | tf_op jit(solution)/shard_map/all_gather | solution.py:24
  172.5 0.0 copy-done
  172.5 0.0 copy-done.5
  172.5 0.0 copy-done.6
  172.5 3.0 fusion.13
  175.5 0.0 copy-done.7
  175.5 6.3 %convolution_convert_fusion.2 = bf16[320,2048]{1,0:T(8,128)(2,1)} fusion(bf16[2048,2688]{1,0:T(8,128)(2,1)} %all-gather.2.cloned.1.call-done, f32[320,640]{1,0:T(8,128)S(1)} %fusion.13, f32[640]{0:T(1024)S(1)} %copy-done.7, bf16[320,2048]{1,0:T(8,128)(2,1)S(1)} %copy-done, f32[2048]{0:T(1024)S(1)} %copy-done.5, f32[320]{0:T(512)S(1)} %add_rsqrt_fusion.1), kind=kOutput, calls=%fused_computation.4 | convolution fusion | flops 1682432000 | bytes 8695552 | tf_op jit(solution)/shard_map/dot_general | solution.py:101
  181.8 0.0 all-to-all-done
  181.8 23.8 %all-to-all-start.1 = ((bf16[8,40,2048]{2,1,0:T(8,128)(2,1)}), bf16[8,40,2048]{2,1,0:T(8,128)(2,1)S(1)}, u32[]{:S(2)}, u32[]{:S(2)}) async-start(bf16[8,40,2048]{2,1,0:T(8,128)(2,1)} %bitcast.51), calls=%async_computation.1 | async-start | bytes 2621440 | tf_op jit(solution)/shard_map/all_to_all | solution.py:17
  205.6 0.5 broadcast.100
  206.1 0.6 reduce.1
  206.7 0.1 reshape.95
  206.8 0.1 reshape.87
  206.9 16.5 %all-to-all-done.1 = bf16[8,40,2048]{2,1,0:T(8,128)(2,1)S(1)} async-done(((bf16[8,40,2048]{2,1,0:T(8,128)(2,1)}), bf16[8,40,2048]{2,1,0:T(8,128)(2,1)S(1)}, u32[]{:S(2)}, u32[]{:S(2)}) %all-to-all-start.1) | async-done | bytes 1310752 | tf_op jit(solution)/shard_map/all_to_all | solution.py:17
  223.4 0.2 convert_reduce_fusion.2
  223.6 0.0 copy-start.2
  223.6 0.0 copy-start.8
  223.6 0.2 fusion.68
  223.8 0.0 copy-done.3
  223.8 0.1 fusion.70
  223.9 1.2 broadcast_in_dim.8
  225.1 4.4 %all-to-all-start.2 = ((bf16[8,40,2048]{2,1,0:T(8,128)(2,1)}), bf16[8,40,2048]{2,1,0:T(8,128)(2,1)S(1)}, u32[]{:S(2)}, u32[]{:S(2)}) async-start(bf16[8,40,2048]{2,1,0:T(8,128)(2,1)} %broadcast_in_dim.8), calls=%async_computation.2 | async-start | bytes 2621440 | tf_op jit(solution)/shard_map/all_to_all | solution.py:53
  229.6 0.0 copy-done.2
  229.6 17.8 %all-to-all-done.2 = bf16[8,40,2048]{2,1,0:T(8,128)(2,1)S(1)} async-done(((bf16[8,40,2048]{2,1,0:T(8,128)(2,1)}), bf16[8,40,2048]{2,1,0:T(8,128)(2,1)S(1)}, u32[]{:S(2)}, u32[]{:S(2)}) %all-to-all-start.2) | async-done | bytes 1310752 | tf_op jit(solution)/shard_map/all_to_all | solution.py:53
  247.4 0.0 copy-done.8
  247.4 1.8 fusion.40
  249.2 0.0 copy-done.9
  249.2 0.0 copy-start.10
  249.2 1.7 fusion.43
  250.9 1.3 fusion.138
  252.3 0.1 pad_maximum_fusion
  252.4 8.0 %all_to_all.41 = f32[8,1,640]{2,1,0:T(1,128)S(1)} all-to-all(f32[8,1,640]{2,1,0:T(1,128)S(1)} %broadcast_in_dim.9), channel_id=1, replica_groups=mesh['rep'=2,'fs'=32,'tp'=8] {'tp'}, dimensions={0} | all-to-all | bytes 40960 | tf_op jit(solution)/shard_map/all_to_all | solution.py:53
  260.4 0.1 slice_multiply_fusion.1
  260.5 0.0 copy-done.10
  260.5 1.8 convolution_convert_fusion.1
  262.3 0.0 copy-start.4
  262.3 20.9 %all_to_all.42 = bf16[8,40,2048]{2,1,0:T(8,128)(2,1)S(1)} all-to-all(bf16[8,40,2048]{2,1,0:T(8,128)(2,1)S(1)} %bitcast.54), channel_id=1, replica_groups=mesh['rep'=2,'fs'=32,'tp'=8] {'tp'}, dimensions={0} | all-to-all | bytes 2621440 | tf_op jit(solution)/shard_map/all_to_all | solution.py:17
  283.2 0.2 convert_reduce_fusion.1
  283.4 0.2 fusion.72
  283.6 0.0 copy-done.4
  283.6 0.1 fusion.74
  283.7 0.1 broadcast_in_dim.10
  283.8 21.2 %all_to_all.43 = bf16[8,40,2048]{2,1,0:T(8,128)(2,1)S(1)} all-to-all(bf16[8,40,2048]{2,1,0:T(8,128)(2,1)S(1)} %broadcast_in_dim.10), channel_id=1, replica_groups=mesh['rep'=2,'fs'=32,'tp'=8] {'tp'}, dimensions={0} | all-to-all | bytes 2621440 | tf_op jit(solution)/shard_map/all_to_all | solution.py:53
  305.1 3.8 %fusion.16 = f32[320,640]{1,0:T(8,128)} fusion(bf16[320,2048]{1,0:T(8,128)(2,1)S(1)} %bitcast.55, bf16[2048,2688]{1,0:T(8,128)(2,1)} %all-gather.2.cloned.1.call-done, f32[640]{0:T(1024)S(1)} %copy-done.6), kind=kOutput, calls=%fused_computation.22 | convolution fusion | flops 839065600 | bytes 4753920 | tf_op jit(solution)/shard_map/dot_general | solution.py:82
  308.9 5.4 %convolution_convert_fusion = bf16[320,2048]{1,0:T(8,128)(2,1)S(1)} fusion(bf16[2048,2688]{1,0:T(8,128)(2,1)} %all-gather.2.cloned.1.call-done, bf16[320,2048]{1,0:T(8,128)(2,1)S(1)} %bitcast.56, f32[320,640]{1,0:T(8,128)} %fusion.16, f32[640]{0:T(1024)S(1)} %copy-done.7), kind=kOutput, calls=%fused_computation.2 | convolution fusion | flops 1679810560 | bytes 8686080 | tf_op jit(solution)/shard_map/dot_general | solution.py:101
  314.3 21.2 %all_to_all.44 = bf16[8,40,2048]{2,1,0:T(8,128)(2,1)S(1)} all-to-all(bf16[8,40,2048]{2,1,0:T(8,128)(2,1)S(1)} %bitcast.57), channel_id=1, replica_groups=mesh['rep'=2,'fs'=32,'tp'=8] {'tp'}, dimensions={0} | all-to-all | bytes 2621440 | tf_op jit(solution)/shard_map/all_to_all | solution.py:17
  335.5 0.2 convert_reduce_fusion
  335.8 0.1 broadcast_in_dim.11
  335.9 21.2 %all_to_all.45 = bf16[8,40,2048]{2,1,0:T(8,128)(2,1)S(1)} all-to-all(bf16[8,40,2048]{2,1,0:T(8,128)(2,1)S(1)} %broadcast_in_dim.11), channel_id=1, replica_groups=mesh['rep'=2,'fs'=32,'tp'=8] {'tp'}, dimensions={0} | all-to-all | bytes 2621440 | tf_op jit(solution)/shard_map/all_to_all | solution.py:53
  357.1 1.1 copy.33
  (17 shorter events, 0.2 us)
Async XLA Ops:
  6.5 166.0 %copy-start = (bf16[320,2048]{1,0:T(8,128)(2,1)S(1)}, bf16[320,2048]{1,0:T(8,128)(2,1)}, u32[]{:S(2)}) copy-start(bf16[320,2048]{1,0:T(8,128)(2,1)} %param.18) | copy-start | bytes 3932164
  6.5 166.0 %copy-start.5 = (f32[2048]{0:T(1024)S(1)}, f32[2048]{0:T(1024)}, u32[]{:S(2)}) copy-start(f32[2048]{0:T(1024)} %param.33) | copy-start | bytes 24580
  6.5 166.0 %copy-start.6 = (f32[640]{0:T(1024)S(1)}, f32[640]{0:T(1024)}, u32[]{:S(2)}) copy-start(f32[640]{0:T(1024)} %param.25) | copy-start | bytes 7684
  6.5 165.9 %all-gather.2.cloned.1.call-start = ((), (), s32[]{:S(2)}) async-start(), calls=%async_computation.8 | async-start | bytes 11354112 | tf_op jit(solution)/shard_map/all_gather | solution.py:24
  12.0 0.7 copy-start.1
  14.1 167.6 %all-to-all-start = ((f32[32,1,128]{2,1,0:T(1,128)}), f32[32,1,128]{2,1,0:T(1,128)S(1)}, u32[]{:S(2)}, u32[]{:S(2)}) async-start(f32[32,1,128]{2,1,0:T(1,128)} %reshape.94), calls=%async_computation | async-start | bytes 32768 | tf_op jit(solution)/shard_map/all_to_all | solution.py:33
  29.3 146.2 %copy-start.7 = (f32[640]{0:T(1024)S(1)}, f32[640]{0:T(1024)}, u32[]{:S(2)}) copy-start(f32[640]{0:T(1024)} %param.26) | copy-start | bytes 7684
  181.8 42.0 %copy-start.3 = (f32[2048]{0:T(1024)S(1)}, f32[2048]{0:T(1024)}, u32[]{:S(2)}) copy-start(f32[2048]{0:T(1024)} %param.34) | copy-start | bytes 24580
  181.8 41.6 %all-to-all-start.1 = ((bf16[8,40,2048]{2,1,0:T(8,128)(2,1)}), bf16[8,40,2048]{2,1,0:T(8,128)(2,1)S(1)}, u32[]{:S(2)}, u32[]{:S(2)}) async-start(bf16[8,40,2048]{2,1,0:T(8,128)(2,1)} %bitcast.51), calls=%async_computation.1 | async-start | bytes 2621440 | tf_op jit(solution)/shard_map/all_to_all | solution.py:17
  223.6 6.0 %copy-start.2 = (f32[31,256]{1,0:T(8,128)S(1)}, f32[31,256]{1,0:T(8,128)}, u32[]{:S(2)}) copy-start(f32[31,256]{1,0:T(8,128)} %param.31) | copy-start | bytes 95236
  223.6 23.8 %copy-start.8 = (f32[256]{0:T(256)S(1)}, f32[256]{0:T(256)}, u32[]{:S(2)}) copy-start(f32[256]{0:T(256)} %param.29) | copy-start | bytes 3076
  225.1 22.3 %all-to-all-start.2 = ((bf16[8,40,2048]{2,1,0:T(8,128)(2,1)}), bf16[8,40,2048]{2,1,0:T(8,128)(2,1)S(1)}, u32[]{:S(2)}, u32[]{:S(2)}) async-start(bf16[8,40,2048]{2,1,0:T(8,128)(2,1)} %broadcast_in_dim.8), calls=%async_computation.2 | async-start | bytes 2621440 | tf_op jit(solution)/shard_map/all_to_all | solution.py:53
  247.4 1.8 copy-start.9
  249.2 11.3 %copy-start.10 = (f32[256]{0:T(256)S(1)}, f32[256]{0:T(256)}, u32[]{:S(2)}) copy-start(f32[256]{0:T(256)} %param.32) | copy-start | bytes 3076
  262.3 21.3 %copy-start.4 = (f32[2048]{0:T(1024)S(1)}, f32[2048]{0:T(1024)}, u32[]{:S(2)}) copy-start(f32[2048]{0:T(1024)} %param.35) | copy-start | bytes 24580
Sparse Core Ops, SparseCore 0:
  12.9 159.5 all-gather.1
